TPU v7x, 32 devices: a whole 2x2x4 slice. The times are simulated.
32 devices in a mesh: sp: 8 (over z, core), tp: 4 (over y, x).
Axes of the slice: x: 2, y: 2, z: 4, core: 2. Of those that a mesh axis runs over, the one named last changes fastest.
Arguments:
- residual: bfloat16 [1536, 2048], P('sp'), may hold values from -6 to 6
- query_in: bfloat16 [1536, 2048], P('sp', 'tp'), may hold values from -6 to 6
- value_in: bfloat16 [1536, 2048], P('sp', 'tp'), may hold values from -6 to 6
- forget_fwd: bfloat16 [1536, 2048], P('sp', 'tp'), may hold values from -4.5 to 4.5
- forget_bwd: bfloat16 [1536, 2048], P('sp', 'tp'), may hold values from -4.5 to 4.5
- jumps: float32 [16, 1536], P('tp', 'sp'), may hold values from -2.8 to 0
- gate_gap: float32 [2, 2048], P(None, 'tp'), may hold values from 0 to 0.1
- out_gate: bfloat16 [1536, 2048], P('sp', 'tp'), may hold values from -6 to 6
- head_gain: float32 [2048], P('tp'), may hold values from 0.1 to 1.9
- out_weight: bfloat16 [2048, 2048], P('tp'), may hold values from -0.25 to 0.25
- norm_gain: float32 [2048], replicated, may hold values from 0.1 to 1.9
- route_ids: int32 [1536, 4], P('sp'), may hold values from 0 to 31, all different within a row; in each aligned block of 192 rows (0 to 191, 192 to 383, ...) at most 36 rows name the same one
- route_weights: float32 [1536, 4], P('sp'), may hold values from 0.05 to 0.5
- w_gate: bfloat16 [32, 2048, 4096], P('sp', None, 'tp'), may hold values from -0.375 to 0.375
- w_up: bfloat16 [32, 2048, 4096], P('sp', None, 'tp'), may hold values from -0.375 to 0.375
- w_down: bfloat16 [32, 4096, 2048], P('sp', None, 'tp'), may hold values from -0.09375 to 0.09375
Outputs:
- mixed: bfloat16 [1536, 2048], P('sp', 'tp')
Inputs may be any that keep to these rules, and one draw needn't show every extreme that they name: `route_ids`: in each aligned block of 192 rows each expert is named by at most 36 rows, and by exactly 36 in some block; each row names 4 different experts.
All inputs are finite; a program needn't handle non-finite values.
Results may differ from a plain program's by a relative error of at most 0.024.
Values may be sent and summed in bfloat16 or wider, within the bound.
A program may use at most 128 MiB of HBM per device.

v0:
```python
import math
import jax
import jax.numpy as jnp
from jax import lax
from jax.sharding import PartitionSpec as P

EXPERTS = 32
CAP = 36
highest_precision = lax.Precision.HIGHEST
eps_norm = 1e-06
limit_value = 7.0
alpha_value = 1.702


def entering(x, axis, join, neutral, backward):
    count = lax.axis_size(axis)
    place = lax.axis_index(axis)
    ahead = count - 1 - place if backward else place
    gathered = jax.tree.map(
        lambda a, kind: lax.all_gather(a.astype(kind), axis),
        x,
        jax.tree.map(lambda a: jnp.bfloat16 if a.dtype == jnp.float32 else a.dtype, x),
    )
    state = jax.tree.map(lambda a, e: jnp.zeros_like(a) + jnp.asarray(e, a.dtype), x, neutral)

    def one(hop, state):
        source = count - 1 - hop if backward else hop
        return join(
            state,
            jax.tree.map(
                lambda a, own: lax.dynamic_index_in_dim(a, source, 0, False).astype(own.dtype),
                gathered,
                x,
            ),
        )

    return lax.fori_loop(0, ahead, one, state)


def block_pass(queries, keys_in, values, logs):
    head_rows, head_count, head_width = queries.shape
    block_size = math.gcd(head_rows, 64)
    block_count = head_rows // block_size

    def to_blocks(array):
        return array.reshape(block_count, block_size, head_count, array.shape[-1])

    q_block, k_block, v_block, log_block = (
        to_blocks(queries),
        to_blocks(keys_in),
        to_blocks(values),
        to_blocks(logs),
    )
    decay_sums = jnp.cumsum(log_block, axis=1)
    middle = decay_sums[:, block_size // 2 - 1 : block_size // 2]
    scores = jnp.einsum(
        "nthk,nshk->nhts",
        q_block * jnp.exp(decay_sums - middle),
        k_block * jnp.exp(middle - decay_sums),
        precision=highest_precision,
    )
    lower_mask = jnp.tril(jnp.ones((block_size, block_size), bool))
    within = jnp.einsum(
        "nhts,nshv->nthv", jnp.where(lower_mask, scores, 0.0), v_block, precision=highest_precision
    )
    block_end = decay_sums[:, -1]
    q_start = q_block * jnp.exp(decay_sums)
    k_end = k_block * jnp.exp(block_end[:, None] - decay_sums)

    def advance(current_state, block_items):
        query_segment, key_segment, value_segment, decay_part = block_items
        state_readout = jnp.einsum(
            "qwe,wei->qwi", query_segment, current_state, precision=highest_precision
        )
        current_state = current_state * jnp.exp(decay_part)[:, :, None] + jnp.einsum(
            "foj,fox->ojx", key_segment, value_segment, precision=highest_precision
        )
        return (current_state, state_readout)

    zero_state = jnp.zeros((head_count, head_width, values.shape[-1]), jnp.float32)
    final_state, across = lax.scan(advance, zero_state, (q_start, k_end, v_block, block_end))
    return ((within + across).reshape(head_rows, head_count, -1), final_state)


def combine_states(first_part, second_part):
    return (
        first_part[0] * second_part[0],
        second_part[0][:, :, None] * first_part[1] + second_part[1],
    )


def carried(queries, logs, running_state):
    decayed_state = queries * jnp.exp(jnp.cumsum(logs, axis=0))
    return jnp.einsum("una,nae->une", decayed_state, running_state, precision=highest_precision)


def shards(
    residual,
    query_in,
    value_in,
    forget_fwd,
    forget_bwd,
    jumps,
    gate_gap,
    out_gate,
    head_gain,
    out_weight,
    norm_gain,
    route_ids,
    route_weights,
    w_gate,
    w_up,
    w_down,
):
    head_rows, local_width = query_in.shape
    head_count = jumps.shape[0]
    head_width = local_width // head_count

    def by_head(array):
        return array.astype(jnp.float32).reshape(head_rows, head_count, head_width)

    queries = jax.nn.silu(by_head(query_in))
    values = by_head(value_in)
    jump_rows = jnp.transpose(jumps)[:, :, None]

    def gate_terms(forget_in, gap):
        key_share = gap.reshape(head_count, head_width) * jax.nn.sigmoid(-by_head(forget_in))
        return (key_share, jnp.log1p(-key_share) + jump_rows)

    keys_fwd, logs_fwd = gate_terms(forget_fwd, gate_gap[0])
    keys_bwd, logs_bwd = gate_terms(forget_bwd, gate_gap[1])
    ones_part = jnp.ones((head_count, head_width), jnp.float32)
    zero_part = jnp.zeros((head_count, head_width, head_width), jnp.float32)
    local_fwd, final_fwd = block_pass(queries, keys_fwd, values, logs_fwd)
    summary_fwd = (jnp.exp(jnp.sum(logs_fwd, axis=0)), final_fwd)
    carry_fwd = entering(summary_fwd, "sp", combine_states, (ones_part, zero_part), False)[1]
    flip_queries = jnp.flip(queries, 0)
    flip_logs = jnp.flip(logs_bwd, 0)
    local_bwd, final_bwd = block_pass(
        flip_queries, jnp.flip(keys_bwd, 0), jnp.flip(values, 0), flip_logs
    )
    summary_bwd = (jnp.exp(jnp.sum(logs_bwd, axis=0)), final_bwd)
    carry_bwd = entering(summary_bwd, "sp", combine_states, (ones_part, zero_part), True)[1]
    forward_out = local_fwd + carried(queries, logs_fwd, carry_fwd)
    backward_out = jnp.flip(local_bwd + carried(flip_queries, flip_logs, carry_bwd), 0)
    mixed_heads = forward_out + backward_out
    mean_square = jnp.mean(mixed_heads * mixed_heads, axis=-1, keepdims=True)
    normed = (mixed_heads * lax.rsqrt(mean_square + eps_norm)).reshape(head_rows, local_width)
    gated = (normed * head_gain * jax.nn.silu(out_gate.astype(jnp.float32))).astype(jnp.bfloat16)
    head_terms = jnp.dot(gated, out_weight, preferred_element_type=jnp.float32)
    summed = lax.psum(head_terms.astype(jnp.bfloat16), "tp").astype(jnp.float32)
    stream = (residual.astype(jnp.float32) + summed).astype(jnp.bfloat16)
    stream_f = stream.astype(jnp.float32)
    row_scale = lax.rsqrt(jnp.mean(stream_f * stream_f, axis=-1, keepdims=True) + eps_norm)
    normed_rows = (stream_f * row_scale * norm_gain).astype(jnp.bfloat16)
    top_count = route_ids.shape[1]
    flat_ids = route_ids.reshape(-1)
    one_hot = (flat_ids[:, None] == jnp.arange(EXPERTS, dtype=jnp.int32)[None, :]).astype(jnp.int32)
    slot_rank = jnp.sum((jnp.cumsum(one_hot, axis=0) - 1) * one_hot, axis=1)
    slot_index = flat_ids * CAP + slot_rank
    owner_rows = jnp.arange(head_rows * top_count, dtype=jnp.int32) // top_count
    slot_rows = jnp.full((EXPERTS * CAP,), head_rows, jnp.int32).at[slot_index].set(owner_rows)
    padded_rows = jnp.concatenate(
        [normed_rows, jnp.zeros((1, normed_rows.shape[1]), jnp.bfloat16)], axis=0
    )
    tp_index = lax.axis_index("tp")
    part_width = w_down.shape[2]
    column_rows = lax.dynamic_slice_in_dim(padded_rows, tp_index * part_width, part_width, 1)
    buffer = column_rows[slot_rows].reshape(EXPERTS, CAP, part_width)
    arrived = lax.all_to_all(buffer, "sp", split_axis=0, concat_axis=1, tiled=True)
    piece = lax.all_gather(arrived, "tp", axis=2, tiled=True)
    gate_sum = jnp.einsum("esd,edf->esf", piece, w_gate, preferred_element_type=jnp.float32)
    up_sum = jnp.einsum("esd,edf->esf", piece, w_up, preferred_element_type=jnp.float32)
    gate_sum = jnp.minimum(gate_sum, limit_value)
    up_sum = jnp.clip(up_sum, -limit_value, limit_value)
    active = (gate_sum * jax.nn.sigmoid(alpha_value * gate_sum) * (up_sum + 1.0)).astype(
        jnp.bfloat16
    )
    produced = jnp.einsum(
        "esf,efd->esd",
        lax.all_gather(active, "tp", axis=2, tiled=True),
        w_down,
        preferred_element_type=jnp.float32,
    ).astype(jnp.bfloat16)
    returned = lax.all_to_all(produced, "sp", split_axis=1, concat_axis=0, tiled=True)
    picked = returned.reshape(EXPERTS * CAP, part_width)[slot_index].astype(jnp.float32)
    picked = picked.reshape(head_rows, top_count, part_width)
    moe_out = jnp.sum(picked * route_weights[:, :, None], axis=1)
    own_columns = lax.dynamic_slice_in_dim(stream_f, tp_index * part_width, part_width, 1)
    return (own_columns + moe_out).astype(jnp.bfloat16)


def solution(mesh):
    return jax.shard_map(
        shards,
        mesh=mesh,
        in_specs=(
            P("sp", None),
            P("sp", "tp"),
            P("sp", "tp"),
            P("sp", "tp"),
            P("sp", "tp"),
            P("tp", "sp"),
            P(None, "tp"),
            P("sp", "tp"),
            P("tp"),
            P("tp", None),
            P(),
            P("sp", None),
            P("sp", None),
            P("sp", None, "tp"),
            P("sp", None, "tp"),
            P("sp", None, "tp"),
        ),
        out_specs=P("sp", "tp"),
        check_vma=False,
    )
```

profile of v0, /device:TPU:0, one launch (start us, length us, event | category | flops | bytes accessed | tf_op | source)
XLA Modules:
  0.0 458.2 jit_solution(397519966608035810)
XLA Ops:
  12.4 2.5 log-plus-one_add_fusion
  32.4 2.7 exponential_multiply_fusion.3
  35.9 10.8 %while.55 = (s32[]{:T(128)}, f32[4,128,128]{2,1,0:T(8,128)S(1)}, f32[3,64,4,128]{3,1,2,0:T(8,128)}, f32[3,4,128]{2,1,0:T(4,128)S(1)}, f32[3,64,4,128]{3,2,1,0:T(...) while((s32[]{:T(128)}, f32[4,128,128]{2,1,0:T(8,128)S(1)}, ...), condition=%wide.region_10.11_spmd.clone, body=%wide.region_9.10_spmd.clone.sunk | while | flops 100925440 | bytes 1842288 | solution.py:81
  54.3 10.9 %while.54 = (s32[]{:T(128)}, f32[4,128,128]{2,1,0:T(8,128)S(1)}, f32[3,64,4,128]{3,1,2,0:T(8,128)}, f32[3,4,128]{2,1,0:T(4,128)S(1)}, f32[3,64,4,128]{3,2,1,0:T(...) while((s32[]{:T(128)}, f32[4,128,128]{2,1,0:T(8,128)S(1)}, ...), condition=%wide.region_2.3_spmd.clone, body=%wide.region_1.2_spmd.clone.sunk | while | flops 100925440 | bytes 2103924 | solution.py:81
  73.4 13.7 %all_gather.29 = bf16[8,4,128]{2,1,0:T(4,128)(2,1)S(1)} all-gather(bf16[1,4,128]{2,1,0:T(4,128)(2,1)S(1)} %fusion.59), channel_id=1, replica_groups=mesh['sp'=8,'tp'=4] {'sp'}, dimensions={0}, use_global_device_ids=true | all-gather | bytes 9216 | tf_op jit(solution)/shard_map/all_gather | solution.py:20
  93.3 8.7 %all_gather.26 = bf16[8,4,128]{2,1,0:T(4,128)(2,1)S(1)} all-gather(bf16[1,4,128]{2,1,0:T(4,128)(2,1)S(1)} %fusion.58), channel_id=1, replica_groups=mesh['sp'=8,'tp'=4] {'sp'}, dimensions={0}, use_global_device_ids=true | all-gather | bytes 9216 | tf_op jit(solution)/shard_map/all_gather | solution.py:20
  102.0 3.0 reduce-window.26
  105.6 7.9 %while.53 = (s32[]{:T(128)}, f32[4,128,128]{2,1,0:T(8,128)S(1)}, s32[]{:T(128)}, bf16[8,4,128]{2,1,0:T(4,128)(2,1)S(1)}, bf16[8,4,128,128]{3,2,1,0:T(8,128)(2,1)...) while((s32[]{:T(128)}, f32[4,128,128]{2,1,0:T(8,128)S(1)}, s32[]{:T(128)}, ...), condition=%wide.region_13.14_spmd, body=%wide.region_12.13_spmd.sunk | while | flops 197126 | bytes 660627 | solution.py:37
  115.8 3.6 rev.20
  120.2 2.6 convolution_convert_fusion
  123.6 3.4 scatter_custom_fusion
  127.0 43.9 %all-reduce.5.cloned.1.call-done = bf16[192,2048]{1,0:T(8,128)(2,1)} async-done(((bf16[192,2048]{1,0:T(8,128)(2,1)}), bf16[192,2048]{1,0:T(8,128)(2,1)}) %all-reduce.5.cloned.1.call-update) | async-done | bytes 786448 | tf_op jit(solution)/shard_map/psum | solution.py:151
  170.9 2.7 fusion.18
  174.0 4.2 gather_fusion
  178.5 36.6 %all_to_all.33 = bf16[32,36,512]{2,1,0:T(8,128)(2,1)S(1)} all-to-all(bf16[32,36,512]{2,1,0:T(8,128)(2,1)S(1)} %reshape.243), channel_id=1, replica_groups=mesh['sp'=8,'tp'=4] {'sp'}, dimensions={0} | all-to-all | bytes 2359296 | tf_op jit(solution)/shard_map/all_to_all | solution.py:170
  217.3 54.6 %all-gather.7.cloned.1.call-done = bf16[4,288,2048]{2,1,0:T(8,128)(2,1)} async-done(((bf16[4,288,512]{2,1,0:T(8,128)(2,1)}), bf16[4,288,2048]{2,1,0:T(8,128)(2,1)}) %all-gather.7.cloned.1.call-update) | async-done | bytes 4718608 | tf_op jit(solution)/shard_map/all_gather | solution.py:171
  272.0 10.2 %fusion.64 = f32[4,288,1024]{2,1,0:T(8,128)S(1)} fusion(bf16[4,288,2048]{2,1,0:T(8,128)(2,1)} %all-gather.7.cloned.1.call-done, bf16[4,2048,1024]{2,1,0:T(8,128)(2,1)} %param.38), kind=kOutput, calls=%fused_computation.155 | convolution fusion | flops 4831838208 | bytes 26214400 | tf_op jit(solution)/shard_map/esd,edf->esf/dot_general | solution.py:173
  282.2 14.0 %multiply_convert_fusion = bf16[4,288,1024]{2,1,0:T(8,128)(2,1)} fusion(f32[4,288,1024]{2,1,0:T(8,128)S(1)} %fusion.64, bf16[4,288,2048]{2,1,0:T(8,128)(2,1)S(1)} %copy-done.24, bf16[4,2048,1024]{2,1,0:T(8,128)(2,1)} %param.37), kind=kOutput, calls=%fused_computation.36 | convolution fusion | flops 4843634688 | bytes 28573696 | tf_op jit(solution)/shard_map/esd,edf->esf/dot_general | solution.py:172
  296.2 96.4 %all-gather.9.cloned.1.call-done = bf16[4,288,4096]{2,1,0:T(8,128)(2,1)} async-done(((bf16[4,288,1024]{2,1,0:T(8,128)(2,1)}), bf16[4,288,4096]{2,1,0:T(8,128)(2,1)}) %all-gather.9.cloned.1.call-update) | async-done | bytes 9437200 | tf_op jit(solution)/shard_map/all_gather | solution.py:181
  392.6 12.5 %convolution_convert_fusion.1 = bf16[4,288,512]{2,1,0:T(8,128)(2,1)S(1)} fusion(bf16[4,288,4096]{2,1,0:T(8,128)(2,1)} %all-gather.9.cloned.1.call-done, bf16[4,4096,512]{2,1,0:T(8,128)(2,1)} %param.39), kind=kOutput, calls=%fused_computation.42 | convolution fusion | flops 4832428032 | bytes 27394048 | tf_op jit(solution)/shard_map/esf,efd->esd/dot_general | solution.py:179
  407.0 4.6 %all-to-all-start.1 = ((bf16[4,288,512]{2,0,1:T(4,128)(2,1)}), bf16[4,288,512]{2,0,1:T(4,128)(2,1)S(1)}, u32[]{:S(2)}, u32[]{:S(2)}) async-start(bf16[4,288,512]{2,0,1:T(4,128)(2,1)} %copy.132), calls=%async_computation.1 | async-start | bytes 2359296 | tf_op jit(solution)/shard_map/all_to_all | solution.py:185
  411.7 29.2 %all-to-all-done.1 = bf16[4,288,512]{2,0,1:T(4,128)(2,1)S(1)} async-done(((bf16[4,288,512]{2,0,1:T(4,128)(2,1)}), bf16[4,288,512]{2,0,1:T(4,128)(2,1)S(1)}, u32[]{:S(2)}, u32[]{:S(2)}) %all-to-all-start.1) | async-done | bytes 1179680 | tf_op jit(solution)/shard_map/all_to_all | solution.py:185
  441.5 3.3 gather_fusion.1
  444.8 2.6 reshape.249
  (195 shorter events, 88.9 us)
Async XLA Ops:
  6.5 113.6 %copy-start = (bf16[512,2048]{1,0:T(8,128)(2,1)S(1)}, bf16[512,2048]{1,0:T(8,128)(2,1)}, u32[]{:S(2)}) copy-start(bf16[512,2048]{1,0:T(8,128)(2,1)} %param.33) | copy-start | bytes 6291460
  6.5 99.1 %all-gather.13.cloned.1.call-start = ((), (), s32[]{:S(2)}) async-start(), calls=%async_computation.6 | async-start | bytes 1179648 | tf_op jit(solution)/shard_map/all_gather | solution.py:20
  7.5 7.4 %copy-start.10 = (f32[192,4]{1,0:T(8,128)}, f32[192,4]{1,0:T(8,128)S(1)}, u32[]{:S(2)}) copy-start(f32[192,4]{1,0:T(8,128)S(1)} %copy.135) | copy-start | bytes 9220
  14.9 7.6 %copy-start.4 = (f32[192,4,128]{2,1,0:T(4,128)}, f32[192,4,128]{2,1,0:T(4,128)S(1)}, u32[]{:S(2)}) copy-start(f32[192,4,128]{2,1,0:T(4,128)S(1)} %get-tuple-element.371) | copy-start | bytes 1179652
  14.9 3.7 copy-start.15
  21.6 10.0 %copy-start.2 = (f32[192,4,128]{2,1,0:T(4,128)}, f32[192,4,128]{2,1,0:T(4,128)S(1)}, u32[]{:S(2)}) copy-start(f32[192,4,128]{2,1,0:T(4,128)S(1)} %get-tuple-element.370) | copy-start | bytes 1179652
  24.5 4.3 copy-start.9
  47.4 72.0 %all-gather.11.cloned.1.call-start = ((), (), s32[]{:S(2)}) async-start(), calls=%async_computation.5 | async-start | bytes 1179648 | tf_op jit(solution)/shard_map/all_gather | solution.py:20
  54.3 13.4 %copy-start.5 = (f32[192,4,128]{2,1,0:T(4,128)S(1)}, f32[192,4,128]{2,1,0:T(4,128)}, u32[]{:S(2)}) copy-start(f32[192,4,128]{2,1,0:T(4,128)} %copy-done.4) | copy-start | bytes 1179652
  54.3 14.2 %copy-start.18 = (s32[192,4]{0,1:T(4,128)S(1)}, s32[192,4]{0,1:T(4,128)}, u32[]{:S(2)}) copy-start(s32[192,4]{0,1:T(4,128)} %param.35) | copy-start | bytes 9220
  65.9 105.0 %all-reduce.5.cloned.1.call-start = ((), (), s32[]{:S(2)}) async-start(), calls=%async_computation.2 | async-start | bytes 1572864 | tf_op jit(solution)/shard_map/psum | solution.py:151
  69.3 19.6 %copy-start.13 = (f32[3,64,4,128]{3,1,2,0:T(8,128)S(1)}, f32[3,64,4,128]{3,1,2,0:T(8,128)}, u32[]{:S(2)}) copy-start(f32[3,64,4,128]{3,1,2,0:T(8,128)} %get-tuple-element.212) | copy-start | bytes 1179652
  91.8 10.2 %copy-start.17 = (s32[6,128]{1,0:T(8,128)S(1)}, s32[6,128]{1,0:T(8,128)}, u32[]{:S(2)}) copy-start(s32[6,128]{1,0:T(8,128)} %eq.29) | copy-start | bytes 9220
  91.8 13.2 %copy-start.19 = (s32[192,4]{0,1:T(4,128)S(1)}, s32[192,4]{0,1:T(4,128)}, u32[]{:S(2)}) copy-start(s32[192,4]{0,1:T(4,128)} %param.35) | copy-start | bytes 9220
  92.4 21.2 %copy-start.12 = (f32[3,64,4,128]{3,1,0,2:T(8,128)S(1)}, f32[3,64,4,128]{3,1,0,2:T(8,128)}, u32[]{:S(2)}) copy-start(f32[3,64,4,128]{3,1,0,2:T(8,128)} %copy.118) | copy-start | bytes 1179652
  115.8 3.7 copy-start.11
  120.2 50.7 %copy-start.6 = (bf16[192,2048]{1,0:T(8,128)(2,1)S(1)}, bf16[192,2048]{1,0:T(8,128)(2,1)}, u32[]{:S(2)}) copy-start(bf16[192,2048]{1,0:T(8,128)(2,1)} %param.24) | copy-start | bytes 2359300
  122.8 50.9 %copy-start.21 = (f32[2048]{0:T(1024)S(1)}, f32[2048]{0:T(1024)}, u32[]{:S(2)}) copy-start(f32[2048]{0:T(1024)} %param.34) | copy-start | bytes 24580
  122.8 149.2 %all-gather.7.cloned.1.call-start = ((), (), s32[]{:S(2)}) async-start(), calls=%async_computation.3 | async-start | bytes 5898240 | tf_op jit(solution)/shard_map/all_gather | solution.py:171
  217.1 175.5 %all-gather.9.cloned.1.call-start = ((), (), s32[]{:S(2)}) async-start(), calls=%async_computation.4 | async-start | bytes 11796480 | tf_op jit(solution)/shard_map/all_gather | solution.py:181
  272.0 10.2 %copy-start.24 = (bf16[4,288,2048]{2,1,0:T(8,128)(2,1)S(1)}, bf16[4,288,2048]{2,1,0:T(8,128)(2,1)}, u32[]{:S(2)}) copy-start(bf16[4,288,2048]{2,1,0:T(8,128)(2,1)} %all-gather.7.cloned.1.call-done) | copy-start | bytes 14155780
  405.0 6.5 %copy-start.23 = (f32[192,4]{0,1:T(4,128)S(1)}, f32[192,4]{0,1:T(4,128)}, u32[]{:S(2)}) copy-start(f32[192,4]{0,1:T(4,128)} %param.36) | copy-start | bytes 9220
  407.0 34.0 %all-to-all-start.1 = ((bf16[4,288,512]{2,0,1:T(4,128)(2,1)}), bf16[4,288,512]{2,0,1:T(4,128)(2,1)S(1)}, u32[]{:S(2)}, u32[]{:S(2)}) async-start(bf16[4,288,512]{2,0,1:T(4,128)(2,1)} %copy.132), calls=%async_computation.1 | async-start | bytes 2359296 | tf_op jit(solution)/shard_map/all_to_all | solution.py:185
  441.5 10.1 %copy-start.1 = (bf16[512,2048]{1,0:T(8,128)(2,1)S(1)}, bf16[512,2048]{1,0:T(8,128)(2,1)}, u32[]{:S(2)}) copy-start(bf16[512,2048]{1,0:T(8,128)(2,1)} %param.33) | copy-start | bytes 6291460
  (8 other events, 16.7 us)
Sparse Core Ops, SparseCore 0:
  47.5 24.9 all-gather.12
  74.1 21.7 all-gather.10
  122.9 47.9 all-reduce.4
  217.2 54.7 all-gather.6
  296.3 96.1 all-gather.8
where the time goes:
time: 460 us; the launch traced here: 458 us
  waiting for transfers between devices  224 us (49%)
  matrix products  60.6 us (13%)
  blocking collectives  59 us (13%)
  local copies, waits for them, and re-layouts  58.7 us (13%)
  other arithmetic  36.5 us (8%)
  between operations  13.7 us (3%)
  starting transfers between devices  4.99 us (1%)
    all_gather x1, waiting for transfers between devices, shards(): lax.all_gather(active, 'tp', axis=2, tiled=True)  96.4 us
    all_gather x1, waiting for transfers between devices, shards(): piece = lax.all_gather(arrived, 'tp', axis=2, tiled=True)  54.6 us
    psum x1, waiting for transfers between devices, shards(): summed = lax.psum(head_terms.astype(jnp.bfloat16), 'tp').astype(jnp.float32)  43.9 us
    all_to_all x1, blocking collectives, shards(): lax.all_to_all(buffer, 'sp', split_axis=0, concat_axis=1, tiled=True)  36.6 us
    all_to_all x1, waiting for transfers between devices, shards(): lax.all_to_all(produced, 'sp', split_axis=1, concat_axis=0, tiled=True)  29.2 us
    all_gather x2, blocking collectives, entering(): lax.all_gather(a.astype(kind), axis)  22.4 us
    dot_general x1, matrix products, shards(): jnp.einsum('esd,edf->esf', piece, w_gate, preferred_element_type=jnp.floa...  14 us
    dot_general x1, matrix products, shards(): jnp.einsum('esf,efd->esd', lax.all_gather(active, 'tp', axis=2, tiled=Tru...  12.5 us
  transfers between devices with their start and end apart: 6, of which 4 were waited for; matrix products, arithmetic and copies ran while one was open for 12% of the time, Pallas kernels for 0%

commit v1 on v0

--- a/solution.py
+++ b/solution.py
@@ -10,6 +10,18 @@
 eps_norm = 1e-06
 limit_value = 7.0
 alpha_value = 1.702
+
+
+def ring_product(shard, axis, dim, term):
+    size, mine, extent = (lax.axis_size(axis), lax.axis_index(axis), shard.shape[dim])
+    right = [(i, (i + 1) % size) for i in range(size)]
+    block, so_far = (shard, None)
+    for step in range(size):
+        coming = lax.ppermute(block, axis, right) if step < size - 1 else None
+        absorb = term(block, (mine - step) % size * extent)
+        so_far = absorb if so_far is None else so_far + absorb
+        block = coming
+    return so_far
 
 
 def entering(x, axis, join, neutral, backward):
@@ -176,11 +188,16 @@
     active = (gate_sum * jax.nn.sigmoid(alpha_value * gate_sum) * (up_sum + 1.0)).astype(
         jnp.bfloat16
     )
-    produced = jnp.einsum(
-        "esf,efd->esd",
-        lax.all_gather(active, "tp", axis=2, tiled=True),
-        w_down,
-        preferred_element_type=jnp.float32,
+    produced = ring_product(
+        active,
+        "tp",
+        2,
+        lambda shard, at: jnp.einsum(
+            "esf,efd->esd",
+            shard,
+            lax.dynamic_slice_in_dim(w_down, at, shard.shape[2], axis=1),
+            preferred_element_type=jnp.float32,
+        ),
     ).astype(jnp.bfloat16)
     returned = lax.all_to_all(produced, "sp", split_axis=1, concat_axis=0, tiled=True)
     picked = returned.reshape(EXPERTS * CAP, part_width)[slot_index].astype(jnp.float32)

time: 460 us -> 516 us (1.12)
  waiting for transfers between devices: 224 us -> 273 us
    ppermute x0 -> x3, waiting for transfers between devices: none -> 145 us  [ring_product(): coming = lax.ppermute(block, axis, right) if step < size - 1 else None]
    all_gather x1 -> x0, waiting for transfers between devices: 96.4 us -> none  [shards(): lax.all_gather(active, 'tp', axis=2, tiled=True)]
    dot_general x1 -> x4, matrix products: 12.5 us -> 16.7 us  [shards(): jnp.einsum('esf,efd->esd', shard, lax.dynamic_slice_in_dim(w_down, at, sh...]
  transfers between devices with their start and end apart: 6 -> 8, of which waited for: 4 -> 6; matrix products, arithmetic and copies ran while one was open for 12% -> 13% of each run, Pallas kernels for 0% -> 0%
where the time goes in v1:
time: 516 us; the launch traced here: 514 us
  waiting for transfers between devices  273 us (53%)
  matrix products  63.7 us (12%)
  local copies, waits for them, and re-layouts  61.4 us (12%)
  blocking collectives  59 us (11%)
  other arithmetic  36.3 us (7%)
  between operations  13.8 us (3%)
  starting transfers between devices  6.8 us (1%)
    ppermute x3, waiting for transfers between devices, ring_product(): coming = lax.ppermute(block, axis, right) if step < size - 1 else None  145 us
    all_gather x1, waiting for transfers between devices, shards(): piece = lax.all_gather(arrived, 'tp', axis=2, tiled=True)  54.9 us
    psum x1, waiting for transfers between devices, shards(): summed = lax.psum(head_terms.astype(jnp.bfloat16), 'tp').astype(jnp.float32)  44 us
    all_to_all x1, blocking collectives, shards(): lax.all_to_all(buffer, 'sp', split_axis=0, concat_axis=1, tiled=True)  36.6 us
    all_to_all x1, waiting for transfers between devices, shards(): lax.all_to_all(produced, 'sp', split_axis=1, concat_axis=0, tiled=True)  29.2 us
    all_gather x2, blocking collectives, entering(): lax.all_gather(a.astype(kind), axis)  22.4 us
    dot_general x4, matrix products, shards(): jnp.einsum('esf,efd->esd', shard, lax.dynamic_slice_in_dim(w_down, at, sh...  16.7 us
    dot_general x1, matrix products, shards(): jnp.einsum('esd,edf->esf', piece, w_gate, preferred_element_type=jnp.floa...  13 us
  transfers between devices with their start and end apart: 8, of which 6 were waited for; matrix products, arithmetic and copies ran while one was open for 13% of the time, Pallas kernels for 0%

profile of v1, /device:TPU:0, one launch (start us, length us, event | category | flops | bytes accessed | tf_op | source)
XLA Modules:
  0.0 514.3 jit_solution(364080091677621628)
XLA Ops:
  35.8 10.7 %while.55 = (s32[]{:T(128)}, f32[4,128,128]{2,1,0:T(8,128)S(1)}, f32[3,64,4,128]{3,1,2,0:T(8,128)}, f32[3,4,128]{2,1,0:T(4,128)S(1)}, f32[3,64,4,128]{3,2,1,0:T(...) while((s32[]{:T(128)}, f32[4,128,128]{2,1,0:T(8,128)S(1)}, ...), condition=%wide.region_10.11_spmd.clone, body=%wide.region_9.10_spmd.clone.sunk | while | flops 100925440 | bytes 1842288 | solution.py:93
  54.1 10.9 %while.54 = (s32[]{:T(128)}, f32[4,128,128]{2,1,0:T(8,128)S(1)}, f32[3,64,4,128]{3,1,2,0:T(8,128)}, f32[3,4,128]{2,1,0:T(4,128)S(1)}, f32[3,64,4,128]{3,2,1,0:T(...) while((s32[]{:T(128)}, f32[4,128,128]{2,1,0:T(8,128)S(1)}, ...), condition=%wide.region_2.3_spmd.clone, body=%wide.region_1.2_spmd.clone.sunk | while | flops 100925440 | bytes 2103924 | solution.py:93
  73.2 13.7 %all_gather.26 = bf16[8,4,128]{2,1,0:T(4,128)(2,1)S(1)} all-gather(bf16[1,4,128]{2,1,0:T(4,128)(2,1)S(1)} %fusion.73), channel_id=1, replica_groups=mesh['sp'=8,'tp'=4] {'sp'}, dimensions={0}, use_global_device_ids=true | all-gather | bytes 9216 | tf_op jit(solution)/shard_map/all_gather | solution.py:32
  93.1 8.7 %all_gather.23 = bf16[8,4,128]{2,1,0:T(4,128)(2,1)S(1)} all-gather(bf16[1,4,128]{2,1,0:T(4,128)(2,1)S(1)} %fusion.72), channel_id=1, replica_groups=mesh['sp'=8,'tp'=4] {'sp'}, dimensions={0}, use_global_device_ids=true | all-gather | bytes 9216 | tf_op jit(solution)/shard_map/all_gather | solution.py:32
  101.8 3.0 reduce-window.26
  105.4 7.9 %while.53 = (s32[]{:T(128)}, f32[4,128,128]{2,1,0:T(8,128)S(1)}, s32[]{:T(128)}, bf16[8,4,128]{2,1,0:T(4,128)(2,1)S(1)}, bf16[8,4,128,128]{3,2,1,0:T(8,128)(2,1)...) while((s32[]{:T(128)}, f32[4,128,128]{2,1,0:T(8,128)S(1)}, s32[]{:T(128)}, ...), condition=%wide.region_13.14_spmd, body=%wide.region_12.13_spmd.sunk | while | flops 197126 | bytes 660627 | solution.py:49
  115.6 3.6 rev.20
  123.4 3.4 scatter_custom_fusion
  126.8 44.0 %all-reduce.5.cloned.1.call-done = bf16[192,2048]{1,0:T(8,128)(2,1)} async-done(((bf16[192,2048]{1,0:T(8,128)(2,1)}), bf16[192,2048]{1,0:T(8,128)(2,1)}) %all-reduce.5.cloned.1.call-update) | async-done | bytes 786448 | tf_op jit(solution)/shard_map/psum | solution.py:163
  173.7 4.2 gather_fusion
  178.3 36.6 %all_to_all.33 = bf16[32,36,512]{2,1,0:T(8,128)(2,1)S(1)} all-to-all(bf16[32,36,512]{2,1,0:T(8,128)(2,1)S(1)} %reshape.243), channel_id=1, replica_groups=mesh['sp'=8,'tp'=4] {'sp'}, dimensions={0} | all-to-all | bytes 2359296 | tf_op jit(solution)/shard_map/all_to_all | solution.py:182
  216.8 54.9 %all-gather.6.cloned.1.call-done = bf16[4,288,2048]{2,1,0:T(8,128)(2,1)} async-done(((bf16[4,288,512]{2,1,0:T(8,128)(2,1)}), bf16[4,288,2048]{2,1,0:T(8,128)(2,1)}) %all-gather.6.cloned.1.call-update) | async-done | bytes 4718608 | tf_op jit(solution)/shard_map/all_gather | solution.py:183
  271.7 10.2 %fusion.78 = f32[4,288,1024]{2,1,0:T(8,128)S(1)} fusion(bf16[4,288,2048]{2,1,0:T(8,128)(2,1)} %all-gather.6.cloned.1.call-done, bf16[4,2048,1024]{2,1,0:T(8,128)(2,1)} %param.38), kind=kOutput, calls=%fused_computation.167 | convolution fusion | flops 4831838208 | bytes 26214400 | tf_op jit(solution)/shard_map/esd,edf->esf/dot_general | solution.py:185
  281.9 13.0 %multiply_convert_fusion = bf16[4,288,1024]{2,1,0:T(8,128)(2,1)S(1)} fusion(f32[4,288,1024]{2,1,0:T(8,128)S(1)} %fusion.78, bf16[4,288,2048]{2,1,0:T(8,128)(2,1)S(1)} %copy-done.27, bf16[4,2048,1024]{2,1,0:T(8,128)(2,1)} %param.37), kind=kOutput, calls=%fused_computation.36 | convolution fusion | flops 4843634688 | bytes 28573696 | tf_op jit(solution)/shard_map/esd,edf->esf/dot_general | solution.py:184
  297.8 52.2 %collective-permute-done = bf16[4,288,1024]{2,1,0:T(8,128)(2,1)S(1)} collective-permute-done((bf16[4,288,1024]{2,1,0:T(8,128)(2,1)S(1)}, bf16[4,288,1024]{2,1,0:T(8,128)(2,1)S(1)}, u32[]{:S(2)}, u32[]{:S(2)}) %collective-permute-start) | collective-permute-done | bytes 2359328 | tf_op jit(solution)/shard_map/ppermute | solution.py:20
  352.1 52.4 %collective-permute-done.1 = bf16[4,288,1024]{2,1,0:T(8,128)(2,1)} collective-permute-done((bf16[4,288,1024]{2,1,0:T(8,128)(2,1)S(1)}, bf16[4,288,1024]{2,1,0:T(8,128)(2,1)}, u32[]{:S(2)}, u32[]{:S(2)}) %collective-permute-start.1) | collective-permute-done | bytes 2359328 | tf_op jit(solution)/shard_map/ppermute | solution.py:20
  404.5 4.4 fusion.19
  408.9 3.6 fusion.17
  412.5 4.3 fusion.15
  416.8 40.0 %collective-permute-done.2 = bf16[4,288,1024]{2,1,0:T(8,128)(2,1)} collective-permute-done((bf16[4,288,1024]{2,1,0:T(8,128)(2,1)}, bf16[4,288,1024]{2,1,0:T(8,128)(2,1)}, u32[]{:S(2)}, u32[]{:S(2)}) %collective-permute-start.2) | collective-permute-done | bytes 2359328 | tf_op jit(solution)/shard_map/ppermute | solution.py:20
  456.8 4.4 add_convert_fusion
  463.1 4.6 all-to-all-start.1
  467.9 29.2 %all-to-all-done.1 = bf16[4,288,512]{2,0,1:T(4,128)(2,1)S(1)} async-done(((bf16[4,288,512]{2,0,1:T(4,128)(2,1)}), bf16[4,288,512]{2,0,1:T(4,128)(2,1)S(1)}, u32[]{:S(2)}, u32[]{:S(2)}) %all-to-all-start.1) | async-done | bytes 1179680 | tf_op jit(solution)/shard_map/all_to_all | solution.py:202
  497.7 3.3 gather_fusion.1
  (207 shorter events, 106.3 us)
Async XLA Ops:
  6.5 113.4 %copy-start = (bf16[512,2048]{1,0:T(8,128)(2,1)S(1)}, bf16[512,2048]{1,0:T(8,128)(2,1)}, u32[]{:S(2)}) copy-start(bf16[512,2048]{1,0:T(8,128)(2,1)} %param.33) | copy-start | bytes 6291460
  6.5 98.9 %all-gather.10.cloned.1.call-start = ((), (), s32[]{:S(2)}) async-start(), calls=%async_computation.5 | async-start | bytes 1179648 | tf_op jit(solution)/shard_map/all_gather | solution.py:32
  7.5 7.4 %copy-start.13 = (f32[192,4]{1,0:T(8,128)}, f32[192,4]{1,0:T(8,128)S(1)}, u32[]{:S(2)}) copy-start(f32[192,4]{1,0:T(8,128)S(1)} %copy.135) | copy-start | bytes 9220
  14.8 7.7 %copy-start.4 = (f32[192,4,128]{2,1,0:T(4,128)}, f32[192,4,128]{2,1,0:T(4,128)S(1)}, u32[]{:S(2)}) copy-start(f32[192,4,128]{2,1,0:T(4,128)S(1)} %get-tuple-element.371) | copy-start | bytes 1179652
  21.6 9.9 %copy-start.2 = (f32[192,4,128]{2,1,0:T(4,128)}, f32[192,4,128]{2,1,0:T(4,128)S(1)}, u32[]{:S(2)}) copy-start(f32[192,4,128]{2,1,0:T(4,128)S(1)} %get-tuple-element.370) | copy-start | bytes 1179652
  47.2 72.0 %all-gather.8.cloned.1.call-start = ((), (), s32[]{:S(2)}) async-start(), calls=%async_computation.4 | async-start | bytes 1179648 | tf_op jit(solution)/shard_map/all_gather | solution.py:32
  54.1 13.4 %copy-start.5 = (f32[192,4,128]{2,1,0:T(4,128)S(1)}, f32[192,4,128]{2,1,0:T(4,128)}, u32[]{:S(2)}) copy-start(f32[192,4,128]{2,1,0:T(4,128)} %copy-done.4) | copy-start | bytes 1179652
  54.1 14.2 %copy-start.21 = (s32[192,4]{0,1:T(4,128)S(1)}, s32[192,4]{0,1:T(4,128)}, u32[]{:S(2)}) copy-start(s32[192,4]{0,1:T(4,128)} %param.35) | copy-start | bytes 9220
  65.7 105.0 %all-reduce.5.cloned.1.call-start = ((), (), s32[]{:S(2)}) async-start(), calls=%async_computation.2 | async-start | bytes 1572864 | tf_op jit(solution)/shard_map/psum | solution.py:163
  69.1 19.6 %copy-start.16 = (f32[3,64,4,128]{3,1,2,0:T(8,128)S(1)}, f32[3,64,4,128]{3,1,2,0:T(8,128)}, u32[]{:S(2)}) copy-start(f32[3,64,4,128]{3,1,2,0:T(8,128)} %get-tuple-element.212) | copy-start | bytes 1179652
  91.6 10.2 %copy-start.20 = (s32[6,128]{1,0:T(8,128)S(1)}, s32[6,128]{1,0:T(8,128)}, u32[]{:S(2)}) copy-start(s32[6,128]{1,0:T(8,128)} %eq.34) | copy-start | bytes 9220
  91.6 13.2 %copy-start.22 = (s32[192,4]{0,1:T(4,128)S(1)}, s32[192,4]{0,1:T(4,128)}, u32[]{:S(2)}) copy-start(s32[192,4]{0,1:T(4,128)} %param.35) | copy-start | bytes 9220
  92.2 21.2 %copy-start.15 = (f32[3,64,4,128]{3,1,0,2:T(8,128)S(1)}, f32[3,64,4,128]{3,1,0,2:T(8,128)}, u32[]{:S(2)}) copy-start(f32[3,64,4,128]{3,1,0,2:T(8,128)} %copy.118) | copy-start | bytes 1179652
  120.0 50.7 %copy-start.6 = (bf16[192,2048]{1,0:T(8,128)(2,1)S(1)}, bf16[192,2048]{1,0:T(8,128)(2,1)}, u32[]{:S(2)}) copy-start(bf16[192,2048]{1,0:T(8,128)(2,1)} %param.24) | copy-start | bytes 2359300
  122.6 50.8 %copy-start.24 = (f32[2048]{0:T(1024)S(1)}, f32[2048]{0:T(1024)}, u32[]{:S(2)}) copy-start(f32[2048]{0:T(1024)} %param.34) | copy-start | bytes 24580
  122.6 149.1 %all-gather.6.cloned.1.call-start = ((), (), s32[]{:S(2)}) async-start(), calls=%async_computation.3 | async-start | bytes 5898240 | tf_op jit(solution)/shard_map/all_gather | solution.py:183
  271.7 10.2 %copy-start.27 = (bf16[4,288,2048]{2,1,0:T(8,128)(2,1)S(1)}, bf16[4,288,2048]{2,1,0:T(8,128)(2,1)}, u32[]{:S(2)}) copy-start(bf16[4,288,2048]{2,1,0:T(8,128)(2,1)} %all-gather.6.cloned.1.call-done) | copy-start | bytes 14155780
  296.3 53.7 %collective-permute-start = (bf16[4,288,1024]{2,1,0:T(8,128)(2,1)S(1)}, bf16[4,288,1024]{2,1,0:T(8,128)(2,1)S(1)}, u32[]{:S(2)}, u32[]{:S(2)}) collective-permute-start(bf16[4,288,1024]{2,1,0:T(8,128)(2,1)S(1)} %multiply_convert_fusion), channel_id=1, source_target_pairs={{0,1},{1,2},{2,3},{3,0},{4,5},{5,6},{6,7},{7,4},{8,9},{9,10},{10,1... | collective-permute-start | bytes 7077896 | tf_op jit(solution)/shard_map/ppermute | solution.py:20
  351.5 53.0 %collective-permute-start.1 = (bf16[4,288,1024]{2,1,0:T(8,128)(2,1)S(1)}, bf16[4,288,1024]{2,1,0:T(8,128)(2,1)}, u32[]{:S(2)}, u32[]{:S(2)}) collective-permute-start(bf16[4,288,1024]{2,1,0:T(8,128)(2,1)S(1)} %collective-permute-done), channel_id=1, source_target_pairs={{0,1},{1,2},{2,3},{3,0},{4,5},{5,6},{6,7},{7,4},{8,9},{9,10},{10,1... | collective-permute-start | bytes 7077896 | tf_op jit(solution)/shard_map/ppermute | solution.py:20
  404.5 52.3 %collective-permute-start.2 = (bf16[4,288,1024]{2,1,0:T(8,128)(2,1)}, bf16[4,288,1024]{2,1,0:T(8,128)(2,1)}, u32[]{:S(2)}, u32[]{:S(2)}) collective-permute-start(bf16[4,288,1024]{2,1,0:T(8,128)(2,1)} %collective-permute-done.1), channel_id=1, source_target_pairs={{0,1},{1,2},{2,3},{3,0},{4,5},{5,6},{6,7},{7,4},{8,9},{9,10},{10,1... | collective-permute-start | bytes 7077896 | tf_op jit(solution)/shard_map/ppermute | solution.py:20
  404.5 4.4 copy-start.10
  461.2 6.6 %copy-start.26 = (f32[192,4]{0,1:T(4,128)S(1)}, f32[192,4]{0,1:T(4,128)}, u32[]{:S(2)}) copy-start(f32[192,4]{0,1:T(4,128)} %param.36) | copy-start | bytes 9220
  463.1 34.0 %all-to-all-start.1 = ((bf16[4,288,512]{2,0,1:T(4,128)(2,1)}), bf16[4,288,512]{2,0,1:T(4,128)(2,1)S(1)}, u32[]{:S(2)}, u32[]{:S(2)}) async-start(bf16[4,288,512]{2,0,1:T(4,128)(2,1)} %copy.132), calls=%async_computation.1 | async-start | bytes 2359296 | tf_op jit(solution)/shard_map/all_to_all | solution.py:202
  497.7 10.1 %copy-start.1 = (bf16[512,2048]{1,0:T(8,128)(2,1)S(1)}, bf16[512,2048]{1,0:T(8,128)(2,1)}, u32[]{:S(2)}) copy-start(bf16[512,2048]{1,0:T(8,128)(2,1)} %param.33) | copy-start | bytes 6291460
  (13 other events, 31.2 us)
Sparse Core Ops, SparseCore 0:
  47.3 24.9 all-gather.9
  73.9 21.8 all-gather.7
  122.7 47.9 all-reduce.4
  216.9 54.7 all-gather.5
